TPU v7x, 512 devices: a 4x2x32 block of a 4x8x32 slice. The times are simulated.
512 devices in a mesh: grp: 2 (over y), ep: 64 (over z, core), tp: 4 (over x).
Axes of the slice: x: 4, y: 2, z: 32, core: 2. Of those that a mesh axis runs over, the one named last changes fastest.
The devices are a block of a 4x8x32 slice.
Arguments:
- tokens: bfloat16 [49152, 2048], P(('grp', 'ep'), 'tp'), parts along dimension 0
- group_choice: int32 [49152], P(('grp', 'ep')), parts along dimension 0, may hold values from 0 to 7, as said below
- expert_choice: int32 [49152, 2], P(('grp', 'ep')), parts along dimension 0, may hold values from 0 to 7, as said below
- group_weight: float32 [49152], P(('grp', 'ep')), parts along dimension 0, may hold values from 0.3 to 1
- expert_weight: float32 [49152, 2], P(('grp', 'ep')), parts along dimension 0, may hold values from 0.1 to 1
- norm_gain: float32 [2048], replicated, may hold values from 0.1 to 1.9
- w_gate: bfloat16 [64, 2048, 1024], P('ep', None, 'tp'), may hold values from -0.125 to 0.125
- w_up: bfloat16 [64, 2048, 1024], P('ep', None, 'tp'), may hold values from -0.125 to 0.125
- w_down: bfloat16 [64, 1024, 2048], P('ep', None, 'tp'), may hold values from -0.1875 to 0.1875
Outputs:
- moe_out: bfloat16 [49152, 2048], P(('grp', 'ep'), 'tp'), parts along dimension 0
There are 2 independent parts, one for each index of `grp`. A program takes and returns all parts, laid end to end along the dimension named above; an argument that names none is the same for every part. Nothing has to cross between parts.
Inputs may be any that keep to these rules, and one draw needn't show every extreme that they name: `group_choice`: group of each token, 0 to 7; within each aligned block of 384 tokens (the tokens of one index of ep) every group is chosen by the same number of tokens. `expert_choice`: a token's two entries differ; within each aligned block of 384 tokens no expert (group with entry) is named by more than 18 tokens, and in every block one expert of each group, the same one in all blocks, is named by exactly 18 tokens.
All inputs are finite; a program needn't handle non-finite values.
Results may differ from a plain program's by a relative error of at most 0.0071.
Values may be sent and summed in bfloat16 or wider, within the bound.
A program may use at most 64 MiB of HBM per device.

v0:
```python
import jax
import jax.numpy as jnp
from jax import lax
from jax.sharding import Mesh
from jax.sharding import PartitionSpec as P

GRP_EP = ("grp", "g", "e")
EP = ("g", "e")
GROUP_SIZE = 8


def rank_before(marks):
    return jnp.cumsum(marks, -2) - marks


def body(
    tokens,
    group_choice,
    expert_choice,
    group_weight,
    expert_weight,
    norm_gain,
    w_gate,
    w_up,
    w_down,
):
    rows, width = tokens.shape
    groups = lax.axis_size("g")
    members = lax.axis_size("e")
    per_group = rows // groups
    mean_load = 2 * per_group // members
    capacity = mean_load + min(mean_load // 2, per_group - mean_load)
    model_width = norm_gain.shape[0]
    mixing = group_weight[:, None] * expert_weight / jnp.sum(expert_weight, -1, keepdims=True)
    group_marks = (group_choice[:, None] == jnp.arange(groups, dtype=jnp.int32)).astype(jnp.int32)
    place = group_choice * per_group + jnp.sum(rank_before(group_marks) * group_marks, 1)
    spots = jnp.arange(rows, dtype=jnp.int32)
    sort = spots[:, None] == place[None, :]
    values = tokens.astype(jnp.float32)
    squares = lax.all_gather(jnp.sum(values * values, -1), "tp", axis=0)
    inv_rms = lax.rsqrt(jnp.sum(squares, 0) / model_width + 1e-06)
    gain = lax.dynamic_slice_in_dim(norm_gain, lax.axis_index("tp") * width, width, 0)
    normed = (values * inv_rms[:, None] * gain[None, :]).astype(jnp.bfloat16)
    by_group = jnp.dot(
        sort.astype(jnp.bfloat16), normed, preferred_element_type=jnp.float32
    ).astype(jnp.bfloat16)
    facts = jnp.concatenate([expert_choice.astype(jnp.float32), mixing], -1)
    facts = jnp.dot(sort.astype(jnp.float32), facts, precision=lax.Precision.HIGHEST)
    landed = lax.all_to_all(
        by_group.reshape(groups, per_group, width), "g", 0, 0, tiled=True
    ).reshape(rows, width)
    facts = lax.all_to_all(facts.reshape(groups, per_group, 4), "g", 0, 0, tiled=True).reshape(
        rows, 4
    )
    chosen = facts[:, :2].astype(jnp.int32).reshape(groups, per_group, 2)
    blocks = jnp.arange(groups, dtype=jnp.int32)[:, None, None]
    kinds = jnp.arange(members, dtype=jnp.int32)
    marks = jnp.sum((chosen[..., None] == kinds).astype(jnp.int32), 2)
    ranks = rank_before(marks)
    seats = jnp.sum(jnp.where(chosen[..., None] == kinds, ranks[:, :, None, :], 0), -1)
    targets = (chosen * groups + blocks) * capacity + seats
    targets = targets.reshape(rows, 2)
    seats_all = members * groups * capacity
    places = jnp.arange(seats_all, dtype=jnp.int32)
    picks = [targets[None, :, k] == places[:, None] for k in range(2)]
    dispatch = (picks[0] | picks[1]).astype(jnp.bfloat16)
    buffer = jnp.dot(dispatch, landed, preferred_element_type=jnp.float32).astype(jnp.bfloat16)
    received = lax.all_to_all(
        buffer.reshape(members, groups * capacity, width), "e", 0, 0, tiled=True
    ).reshape(seats_all, width)
    piece = lax.all_gather(received, "tp", axis=1, tiled=True)
    gate = jnp.dot(piece, w_gate[0], preferred_element_type=jnp.float32)
    up = jnp.dot(piece, w_up[0], preferred_element_type=jnp.float32)
    hidden = (jax.nn.silu(gate) * up).astype(jnp.bfloat16)
    hidden = lax.all_gather(hidden, "tp", axis=1, tiled=True)
    result = jnp.dot(hidden, w_down[0], preferred_element_type=jnp.float32).astype(jnp.bfloat16)
    back = lax.all_to_all(
        result.reshape(members, groups * capacity, width), "e", 0, 0, tiled=True
    ).reshape(seats_all, width)
    mixed = jnp.zeros((rows, width), jnp.float32)
    for k in range(2):
        picker = (targets[:, k : k + 1] == places[None, :]).astype(jnp.bfloat16)
        picked = jnp.dot(picker, back, preferred_element_type=jnp.float32)
        mixed = mixed + facts[:, 2 + k : 3 + k] * picked
    home = lax.all_to_all(
        mixed.astype(jnp.bfloat16).reshape(groups, per_group, width), "g", 0, 0, tiled=True
    ).reshape(rows, width)
    unsort = place[:, None] == spots[None, :]
    return jnp.dot(unsort.astype(jnp.bfloat16), home, preferred_element_type=jnp.float32).astype(
        jnp.bfloat16
    )


def solution(mesh):
    members = GROUP_SIZE
    split = Mesh(
        mesh.devices.reshape(
            mesh.shape["grp"], mesh.shape["ep"] // members, members, mesh.shape["tp"]
        ),
        ("grp", "g", "e", "tp"),
    )
    placed = (
        P(GRP_EP, "tp"),
        P(GRP_EP),
        P(GRP_EP, None),
        P(GRP_EP),
        P(GRP_EP, None),
        P(),
        P(EP, None, "tp"),
        P(EP, None, "tp"),
        P(EP, None, "tp"),
    )
    return jax.shard_map(
        body, mesh=split, in_specs=placed, out_specs=P(GRP_EP, "tp"), check_vma=False
    )
```

profile of v0, /device:TPU:96, one launch (start us, length us, event | category | flops | bytes accessed | tf_op | source)
XLA Modules:
  0.0 404.2 jit_solution(10690738187043938088)
XLA Ops:
  6.6 0.8 convert_element_type.48
  7.3 0.7 fusion.29
  8.0 0.8 reduce-window.6
  8.9 0.2 slice_reduce_fusion
  9.1 0.8 fusion.28
  9.9 0.7 multiply_add_fusion.1
  10.6 0.7 reduce_sum.57
  11.3 0.7 multiply_divide_fusion
  12.0 0.4 fusion.20
  12.4 0.1 reshape.73
  12.5 0.7 reshape.92
  13.2 42.5 %all-to-all-start = ((f32[8,1,192]{2,1,0:T(1,128)}), f32[8,1,192]{2,1,0:T(1,128)S(1)}, u32[]{:S(2)}, u32[]{:S(2)}) async-start(f32[8,1,192]{2,1,0:T(1,128)} %reshape.92), calls=%async_computation | async-start | bytes 16384 | tf_op jit(solution)/shard_map/all_to_all | solution.py:52
  55.7 1.2 fusion.17
  56.9 11.4 %all-gather.1 = f32[4,1,384]{2,1,0:T(1,128)S(1)} all-gather(f32[1,1,384]{2,1,0:T(1,128)S(1)} %reshape.84), channel_id=2, replica_groups=mesh['grp'=2,'g'=8,'e'=8,'tp'=4] {'tp'}, dimensions={0}, use_global_device_ids=true | all-gather | bytes 7680 | tf_op jit(solution)/shard_map/all_gather | solution.py:40
  68.3 0.8 dynamic_slice.3
  69.1 2.2 convolution_convert_fusion.3
  71.3 6.7 %all-to-all-done = f32[8,1,192]{2,1,0:T(1,128)S(1)} async-done(((f32[8,1,192]{2,1,0:T(1,128)}), f32[8,1,192]{2,1,0:T(1,128)S(1)}, u32[]{:S(2)}, u32[]{:S(2)}) %all-to-all-start) | async-done | bytes 6176 | tf_op jit(solution)/shard_map/all_to_all | solution.py:52
  78.0 15.0 %all-to-all-start.1 = ((bf16[8,48,512]{2,1,0:T(8,128)(2,1)}), bf16[8,48,512]{2,1,0:T(8,128)(2,1)S(1)}, u32[]{:S(2)}, u32[]{:S(2)}) async-start(bf16[8,48,512]{2,1,0:T(8,128)(2,1)} %bitcast.3), calls=%async_computation.1 | async-start | bytes 786432 | tf_op jit(solution)/shard_map/all_to_all | solution.py:49
  92.9 0.1 all-gather.5.cloned.1.call-start
  93.0 0.1 add.42
  93.1 0.6 broadcast.44
  93.7 0.7 reduce.11
  94.4 0.1 reshape.93
  94.5 0.1 reshape.74
  94.6 0.1 eq.140
  94.7 0.1 copy.29
  94.8 3.8 reduce-window_subtract_fusion
  98.6 0.1 copy.31
  98.8 0.1 reduce_sum.60
  98.9 34.6 %all-to-all-done.1 = bf16[8,48,512]{2,1,0:T(8,128)(2,1)S(1)} async-done(((bf16[8,48,512]{2,1,0:T(8,128)(2,1)}), bf16[8,48,512]{2,1,0:T(8,128)(2,1)S(1)}, u32[]{:S(2)}, u32[]{:S(2)}) %all-to-all-start.1) | async-done | bytes 393248 | tf_op jit(solution)/shard_map/all_to_all | solution.py:49
  133.6 0.8 convolution_convert_fusion.1
  134.4 40.5 %all_to_all.25 = bf16[8,144,512]{2,1,0:T(8,128)(2,1)} all-to-all(bf16[8,144,512]{2,1,0:T(8,128)(2,1)S(1)} %bitcast.50), channel_id=1, replica_groups=mesh['grp'=2,'g'=8,'e'=8,'tp'=4] {'e'}, dimensions={0} | all-to-all | bytes 2359296 | tf_op jit(solution)/shard_map/all_to_all | solution.py:68
  174.9 0.1 all-gather.5.cloned.1.call-update
  174.9 0.0 copy-start.3
  175.0 0.1 all-gather.7.cloned.1.call-start
  175.0 52.6 %all-gather.5.cloned.1.call-done = bf16[1152,2048]{1,0:T(8,128)(2,1)} async-done(((bf16[1152,512]{1,0:T(8,128)(2,1)}), bf16[1152,2048]{1,0:T(8,128)(2,1)}) %all-gather.5.cloned.1.call-update) | async-done | bytes 4718608 | tf_op jit(solution)/shard_map/all_gather | solution.py:71
  227.7 3.9 fusion.11
  231.6 2.4 fusion
  234.0 0.1 all-gather.7.cloned.1.call-update
  234.0 53.1 %all-gather.7.cloned.1.call-done = bf16[1152,1024]{1,0:T(8,128)(2,1)} async-done(((bf16[1152,256]{1,0:T(8,128)(2,1)}), bf16[1152,1024]{1,0:T(8,128)(2,1)}) %all-gather.7.cloned.1.call-update) | async-done | bytes 2359312 | tf_op jit(solution)/shard_map/all_gather | solution.py:75
  287.2 0.0 copy-done
  287.2 4.1 %convolution_convert_fusion = bf16[1152,512]{1,0:T(8,128)(2,1)} fusion(bf16[1152,1024]{1,0:T(8,128)(2,1)} %all-gather.7.cloned.1.call-done, bf16[1,1024,512]{2,1,0:T(8,128)(2,1)S(1)} %copy-done), kind=kOutput, calls=%fused_computation | convolution fusion | flops 1208549376 | bytes 4587520 | tf_op jit(solution)/shard_map/dot_general | solution.py:76
  291.2 5.3 %all-to-all-start.3 = ((bf16[8,144,512]{2,1,0:T(8,128)(2,1)}), bf16[8,144,512]{2,1,0:T(8,128)(2,1)S(1)}, u32[]{:S(2)}, u32[]{:S(2)}) async-start(bf16[8,144,512]{2,1,0:T(8,128)(2,1)} %bitcast.10), calls=%async_computation.3 | async-start | bytes 2359296 | tf_op jit(solution)/shard_map/all_to_all | solution.py:77
  296.5 25.9 %all-to-all-done.3 = bf16[8,144,512]{2,1,0:T(8,128)(2,1)S(1)} async-done(((bf16[8,144,512]{2,1,0:T(8,128)(2,1)}), bf16[8,144,512]{2,1,0:T(8,128)(2,1)S(1)}, u32[]{:S(2)}, u32[]{:S(2)}) %all-to-all-start.3) | async-done | bytes 1179680 | tf_op jit(solution)/shard_map/all_to_all | solution.py:77
  322.4 0.7 fusion.7
  323.2 0.7 fusion.8
  323.9 72.3 %all_to_all.26 = bf16[8,48,512]{2,1,0:T(8,128)(2,1)S(1)} all-to-all(bf16[8,48,512]{2,1,0:T(8,128)(2,1)S(1)} %bitcast.52), channel_id=1, replica_groups=mesh['grp'=2,'g'=8,'e'=8,'tp'=4] {'g'}, dimensions={0} | all-to-all | bytes 786432 | tf_op jit(solution)/shard_map/all_to_all | solution.py:85
  396.2 1.2 convolution_convert_fusion.2
  (21 shorter events, 0.3 us)
Async XLA Ops:
  6.5 280.6 %copy-start = (bf16[1,1024,512]{2,1,0:T(8,128)(2,1)S(1)}, bf16[1,1024,512]{2,1,0:T(8,128)(2,1)}, u32[]{:S(2)}) copy-start(bf16[1,1024,512]{2,1,0:T(8,128)(2,1)} %param.17) | copy-start | bytes 3145732
  13.2 64.8 %all-to-all-start = ((f32[8,1,192]{2,1,0:T(1,128)}), f32[8,1,192]{2,1,0:T(1,128)S(1)}, u32[]{:S(2)}, u32[]{:S(2)}) async-start(f32[8,1,192]{2,1,0:T(1,128)} %reshape.92), calls=%async_computation | async-start | bytes 16384 | tf_op jit(solution)/shard_map/all_to_all | solution.py:52
  78.0 55.6 %all-to-all-start.1 = ((bf16[8,48,512]{2,1,0:T(8,128)(2,1)}), bf16[8,48,512]{2,1,0:T(8,128)(2,1)S(1)}, u32[]{:S(2)}, u32[]{:S(2)}) async-start(bf16[8,48,512]{2,1,0:T(8,128)(2,1)} %bitcast.3), calls=%async_computation.1 | async-start | bytes 786432 | tf_op jit(solution)/shard_map/all_to_all | solution.py:49
  92.9 134.7 %all-gather.5.cloned.1.call-start = ((), (), s32[]{:S(2)}) async-start(), calls=%async_computation.5 | async-start | bytes 5898240 | tf_op jit(solution)/shard_map/all_gather | solution.py:71
  174.9 52.8 %copy-start.2 = (bf16[1,2048,256]{2,1,0:T(8,128)(2,1)S(1)}, bf16[1,2048,256]{2,1,0:T(8,128)(2,1)}, u32[]{:S(2)}) copy-start(bf16[1,2048,256]{2,1,0:T(8,128)(2,1)} %param.15) | copy-start | bytes 3145732
  174.9 56.6 %copy-start.3 = (bf16[1,2048,256]{2,1,0:T(8,128)(2,1)S(1)}, bf16[1,2048,256]{2,1,0:T(8,128)(2,1)}, u32[]{:S(2)}) copy-start(bf16[1,2048,256]{2,1,0:T(8,128)(2,1)} %param.16) | copy-start | bytes 3145732
  175.0 112.2 %all-gather.7.cloned.1.call-start = ((), (), s32[]{:S(2)}) async-start(), calls=%async_computation.6 | async-start | bytes 2949120 | tf_op jit(solution)/shard_map/all_gather | solution.py:75
  227.7 3.9 copy-start.1
  291.2 31.2 %all-to-all-start.3 = ((bf16[8,144,512]{2,1,0:T(8,128)(2,1)}), bf16[8,144,512]{2,1,0:T(8,128)(2,1)S(1)}, u32[]{:S(2)}, u32[]{:S(2)}) async-start(bf16[8,144,512]{2,1,0:T(8,128)(2,1)} %bitcast.10), calls=%async_computation.3 | async-start | bytes 2359296 | tf_op jit(solution)/shard_map/all_to_all | solution.py:77
Sparse Core Ops, SparseCore 0:
  175.1 52.5 all-gather.4
  234.1 52.9 all-gather.6
where the time goes:
time: 405 us; the launch traced here: 404 us
  waiting for transfers between devices  173 us (43%)
  blocking collectives  124 us (31%)
  starting transfers between devices  62.9 us (16%)
  matrix products  16.3 us (4%)
  between operations  13.6 us (3%)
  other arithmetic  11 us (3%)
    all_to_all x1, blocking collectives, body(): lax.all_to_all(mixed.astype(jnp.bfloat16).reshape(groups, per_group, widt...  72.3 us
    all_gather x1, waiting for transfers between devices, body(): hidden = lax.all_gather(hidden, 'tp', axis=1, tiled=True)  53.1 us
    all_gather x1, waiting for transfers between devices, body(): piece = lax.all_gather(received, 'tp', axis=1, tiled=True)  52.6 us
    all_to_all x1, starting transfers between devices, body(): lax.all_to_all(facts.reshape(groups, per_group, 4), 'g', 0, 0, tiled=True)  42.5 us
    all_to_all x1, blocking collectives, body(): lax.all_to_all(buffer.reshape(members, groups * capacity, width), 'e', 0,...  40.5 us
    all_to_all x1, waiting for transfers between devices, body(): lax.all_to_all(by_group.reshape(groups, per_group, width), 'g', 0, 0, til...  34.6 us
    all_to_all x1, waiting for transfers between devices, body(): lax.all_to_all(result.reshape(members, groups * capacity, width), 'e', 0,...  25.9 us
    all_to_all x1, starting transfers between devices, body(): lax.all_to_all(by_group.reshape(groups, per_group, width), 'g', 0, 0, til...  15 us
  transfers between devices with their start and end apart: 5, of which 5 were waited for; matrix products, arithmetic and copies ran while one was open for 2% of the time, Pallas kernels for 0%

commit v1 on v0

--- a/solution.py
+++ b/solution.py
@@ -7,6 +7,12 @@
 GRP_EP = ("grp", "g", "e")
 EP = ("g", "e")
 GROUP_SIZE = 8
+
+
+def laid_out(blocks, dim):
+    lengths = list(blocks.shape[1:])
+    lengths[dim] *= blocks.shape[0]
+    return jnp.moveaxis(blocks, 0, dim).reshape(lengths)
 
 
 def rank_before(marks):
@@ -72,7 +78,19 @@
     gate = jnp.dot(piece, w_gate[0], preferred_element_type=jnp.float32)
     up = jnp.dot(piece, w_up[0], preferred_element_type=jnp.float32)
     hidden = (jax.nn.silu(gate) * up).astype(jnp.bfloat16)
-    hidden = lax.all_gather(hidden, "tp", axis=1, tiled=True)
+    size = lax.axis_size("tp")
+    pairs = [(i, (i + 1) % size) for i in range(size)]
+    back_2 = [(b, a) for a, b in pairs]
+    lower, upper = ([], [])
+    for lap in range(size - 1):
+        if lap % 2 == 0:
+            lower.append(lax.ppermute(lower[-1] if lower else hidden, "tp", pairs))
+        else:
+            upper.append(lax.ppermute(upper[-1] if upper else hidden, "tp", back_2))
+    blocks_2 = jnp.stack([*lower[::-1], hidden, *upper])
+    shift = lax.axis_index("tp") - len(lower)
+    blocks_2 = blocks_2[(jnp.arange(size) - shift) % size]
+    hidden = laid_out(blocks_2, 1)
     result = jnp.dot(hidden, w_down[0], preferred_element_type=jnp.float32).astype(jnp.bfloat16)
     back = lax.all_to_all(
         result.reshape(members, groups * capacity, width), "e", 0, 0, tiled=True

time: 405 us -> 393 us (0.970)
  waiting for transfers between devices: 173 us -> 146 us
  starting transfers between devices: 62.9 us -> 71.9 us
  local copies, waits for them, and re-layouts: 3.1 us -> 9.05 us
    all_gather x1 -> x0, waiting for transfers between devices: 53.1 us -> none  [body(): hidden = lax.all_gather(hidden, 'tp', axis=1, tiled=True)]
    ppermute x0 -> x3, waiting for transfers between devices: none -> 26.1 us  [the longest x2 26.1 us: body(): lower.append(lax.ppermute(lower[-1] if lower else hidden, 'tp', pairs))]
    ppermute x0 -> x3, starting transfers between devices: none -> 9.05 us  [the longest x2 4.8 us: body(): lower.append(lax.ppermute(lower[-1] if lower else hidden, 'tp', pairs))]
  transfers between devices with their start and end apart: 5 -> 7, of which waited for: 5 -> 6; matrix products, arithmetic and copies ran while one was open for 2% -> 3% of each run, Pallas kernels for 0% -> 0%
where the time goes in v1:
time: 393 us; the launch traced here: 392 us
  waiting for transfers between devices  146 us (37%)
  blocking collectives  124 us (32%)
  starting transfers between devices  71.9 us (18%)
  matrix products  13.9 us (4%)
  between operations  13.7 us (3%)
  other arithmetic  12.9 us (3%)
  local copies, waits for them, and re-layouts  9.05 us (2%)
    all_to_all x1, blocking collectives, body(): lax.all_to_all(mixed.astype(jnp.bfloat16).reshape(groups, per_group, widt...  72.3 us
    all_gather x1, waiting for transfers between devices, body(): piece = lax.all_gather(received, 'tp', axis=1, tiled=True)  52.6 us
    all_to_all x1, starting transfers between devices, body(): lax.all_to_all(facts.reshape(groups, per_group, 4), 'g', 0, 0, tiled=True)  42.5 us
    all_to_all x1, blocking collectives, body(): lax.all_to_all(buffer.reshape(members, groups * capacity, width), 'e', 0,...  40.7 us
    all_to_all x1, waiting for transfers between devices, body(): lax.all_to_all(by_group.reshape(groups, per_group, width), 'g', 0, 0, til...  34.6 us
    ppermute x2, waiting for transfers between devices, body(): lower.append(lax.ppermute(lower[-1] if lower else hidden, 'tp', pairs))  26.1 us
    all_to_all x1, waiting for transfers between devices, body(): lax.all_to_all(result.reshape(members, groups * capacity, width), 'e', 0,...  25.9 us
    all_to_all x1, starting transfers between devices, body(): lax.all_to_all(by_group.reshape(groups, per_group, width), 'g', 0, 0, til...  15 us
  transfers between devices with their start and end apart: 7, of which 6 were waited for; matrix products, arithmetic and copies ran while one was open for 3% of the time, Pallas kernels for 0%

profile of v1, /device:TPU:96, one launch (start us, length us, event | category | flops | bytes accessed | tf_op | source)
XLA Modules:
  0.0 391.8 jit_solution(7656945858088602799)
XLA Ops:
  6.6 0.8 fusion.29
  7.3 0.8 reduce-window.6
  8.2 0.2 slice_reduce_fusion
  8.4 0.8 fusion.28
  9.2 0.7 multiply_add_fusion.1
  9.9 0.7 convert_element_type.48
  10.6 0.7 reduce_sum.57
  11.3 0.7 multiply_divide_fusion
  12.0 0.4 fusion.20
  12.4 0.1 reshape.125
  12.5 0.7 reshape.153
  13.2 42.5 %all-to-all-start = ((f32[8,1,192]{2,1,0:T(1,128)}), f32[8,1,192]{2,1,0:T(1,128)S(1)}, u32[]{:S(2)}, u32[]{:S(2)}) async-start(f32[8,1,192]{2,1,0:T(1,128)} %reshape.153), calls=%async_computation | async-start | bytes 16384 | tf_op jit(solution)/shard_map/all_to_all | solution.py:58
  55.7 1.2 fusion.17
  56.9 11.4 %all-gather.1 = f32[4,1,384]{2,1,0:T(1,128)S(1)} all-gather(f32[1,1,384]{2,1,0:T(1,128)S(1)} %reshape.145), channel_id=2, replica_groups=mesh['grp'=2,'g'=8,'e'=8,'tp'=4] {'tp'}, dimensions={0}, use_global_device_ids=true | all-gather | bytes 7680 | tf_op jit(solution)/shard_map/all_gather | solution.py:46
  68.3 0.8 dynamic_slice.3
  69.1 2.2 convolution_convert_fusion.3
  71.3 6.7 %all-to-all-done = f32[8,1,192]{2,1,0:T(1,128)S(1)} async-done(((f32[8,1,192]{2,1,0:T(1,128)}), f32[8,1,192]{2,1,0:T(1,128)S(1)}, u32[]{:S(2)}, u32[]{:S(2)}) %all-to-all-start) | async-done | bytes 6176 | tf_op jit(solution)/shard_map/all_to_all | solution.py:58
  77.9 15.0 %all-to-all-start.1 = ((bf16[8,48,512]{2,1,0:T(8,128)(2,1)}), bf16[8,48,512]{2,1,0:T(8,128)(2,1)S(1)}, u32[]{:S(2)}, u32[]{:S(2)}) async-start(bf16[8,48,512]{2,1,0:T(8,128)(2,1)} %bitcast.3), calls=%async_computation.1 | async-start | bytes 786432 | tf_op jit(solution)/shard_map/all_to_all | solution.py:55
  93.1 0.6 broadcast.113
  93.7 0.7 reduce.11
  94.5 0.1 reshape.126
  94.6 0.1 eq.142
  94.7 0.1 copy.33
  94.8 3.8 reduce-window_subtract_fusion
  98.6 0.1 copy.35
  98.8 0.1 reduce_sum.60
  98.9 34.6 %all-to-all-done.1 = bf16[8,48,512]{2,1,0:T(8,128)(2,1)S(1)} async-done(((bf16[8,48,512]{2,1,0:T(8,128)(2,1)}), bf16[8,48,512]{2,1,0:T(8,128)(2,1)S(1)}, u32[]{:S(2)}, u32[]{:S(2)}) %all-to-all-start.1) | async-done | bytes 393248 | tf_op jit(solution)/shard_map/all_to_all | solution.py:55
  133.6 0.8 convolution_convert_fusion.1
  134.4 40.7 %all_to_all.25 = bf16[8,144,512]{2,1,0:T(8,128)(2,1)} all-to-all(bf16[8,144,512]{2,1,0:T(8,128)(2,1)S(1)} %bitcast.61), channel_id=1, replica_groups=mesh['grp'=2,'g'=8,'e'=8,'tp'=4] {'e'}, dimensions={0} | all-to-all | bytes 2359296 | tf_op jit(solution)/shard_map/all_to_all | solution.py:74
  175.1 52.6 %all-gather.4.cloned.1.call-done = bf16[1152,2048]{1,0:T(8,128)(2,1)} async-done(((bf16[1152,512]{1,0:T(8,128)(2,1)}), bf16[1152,2048]{1,0:T(8,128)(2,1)}) %all-gather.4.cloned.1.call-update) | async-done | bytes 4718608 | tf_op jit(solution)/shard_map/all_gather | solution.py:77
  227.8 3.9 fusion.11
  231.7 1.6 fusion
  233.2 2.9 collective-permute-start
  236.1 4.2 %collective-permute-start.2 = (bf16[1152,256]{1,0:T(8,128)(2,1)S(1)}, bf16[1152,256]{1,0:T(8,128)(2,1)S(1)}, u32[]{:S(2)}, u32[]{:S(2)}) collective-permute-start(bf16[1152,256]{1,0:T(8,128)(2,1)S(1)} %fusion), channel_id=1, source_target_pairs={{1,0},{2,1},{3,2},{0,3},{5,4},{6,5},{7,6},{4,7},{9,8},{10,9},{11,1... | collective-permute-start | bytes 1769480 | tf_op jit(solution)/shard_map/ppermute | solution.py:89
  240.4 10.9 %collective-permute-done = bf16[1152,256]{1,0:T(8,128)(2,1)S(1)} collective-permute-done((bf16[1152,256]{1,0:T(8,128)(2,1)S(1)}, bf16[1152,256]{1,0:T(8,128)(2,1)S(1)}, u32[]{:S(2)}, u32[]{:S(2)}) %collective-permute-start) | collective-permute-done | bytes 589856 | tf_op jit(solution)/shard_map/ppermute | solution.py:87
  251.3 1.9 collective-permute-start.1
  253.3 15.2 %collective-permute-done.1 = bf16[1152,256]{1,0:T(8,128)(2,1)S(1)} collective-permute-done((bf16[1152,256]{1,0:T(8,128)(2,1)S(1)}, bf16[1152,256]{1,0:T(8,128)(2,1)S(1)}, u32[]{:S(2)}, u32[]{:S(2)}) %collective-permute-start.1) | collective-permute-done | bytes 589856 | tf_op jit(solution)/shard_map/ppermute | solution.py:87
  268.5 0.8 copy-done.4
  269.3 1.9 pad_maximum_fusion
  271.2 2.1 gather_fusion
  273.3 3.0 copy.37
  276.3 2.4 convolution_convert_fusion
  278.8 5.3 %all-to-all-start.3 = ((bf16[8,144,512]{2,1,0:T(8,128)(2,1)}), bf16[8,144,512]{2,1,0:T(8,128)(2,1)S(1)}, u32[]{:S(2)}, u32[]{:S(2)}) async-start(bf16[8,144,512]{2,1,0:T(8,128)(2,1)} %bitcast.60), calls=%async_computation.3 | async-start | bytes 2359296 | tf_op jit(solution)/shard_map/all_to_all | solution.py:95
  284.0 25.9 %all-to-all-done.3 = bf16[8,144,512]{2,1,0:T(8,128)(2,1)S(1)} async-done(((bf16[8,144,512]{2,1,0:T(8,128)(2,1)}), bf16[8,144,512]{2,1,0:T(8,128)(2,1)S(1)}, u32[]{:S(2)}, u32[]{:S(2)}) %all-to-all-start.3) | async-done | bytes 1179680 | tf_op jit(solution)/shard_map/all_to_all | solution.py:95
  309.9 0.7 fusion.7
  310.7 0.7 fusion.8
  311.4 72.3 %all_to_all.26 = bf16[8,48,512]{2,1,0:T(8,128)(2,1)S(1)} all-to-all(bf16[8,48,512]{2,1,0:T(8,128)(2,1)S(1)} %bitcast.67), channel_id=1, replica_groups=mesh['grp'=2,'g'=8,'e'=8,'tp'=4] {'g'}, dimensions={0} | all-to-all | bytes 786432 | tf_op jit(solution)/shard_map/all_to_all | solution.py:103
  383.7 1.2 convolution_convert_fusion.2
  (37 shorter events, 0.6 us)
Async XLA Ops:
  6.5 269.8 %copy-start = (bf16[1,1024,512]{2,1,0:T(8,128)(2,1)S(1)}, bf16[1,1024,512]{2,1,0:T(8,128)(2,1)}, u32[]{:S(2)}) copy-start(bf16[1,1024,512]{2,1,0:T(8,128)(2,1)} %param.17) | copy-start | bytes 3145732
  13.2 64.8 %all-to-all-start = ((f32[8,1,192]{2,1,0:T(1,128)}), f32[8,1,192]{2,1,0:T(1,128)S(1)}, u32[]{:S(2)}, u32[]{:S(2)}) async-start(f32[8,1,192]{2,1,0:T(1,128)} %reshape.153), calls=%async_computation | async-start | bytes 16384 | tf_op jit(solution)/shard_map/all_to_all | solution.py:58
  77.9 55.6 %all-to-all-start.1 = ((bf16[8,48,512]{2,1,0:T(8,128)(2,1)}), bf16[8,48,512]{2,1,0:T(8,128)(2,1)S(1)}, u32[]{:S(2)}, u32[]{:S(2)}) async-start(bf16[8,48,512]{2,1,0:T(8,128)(2,1)} %bitcast.3), calls=%async_computation.1 | async-start | bytes 786432 | tf_op jit(solution)/shard_map/all_to_all | solution.py:55
  92.9 134.8 %all-gather.4.cloned.1.call-start = ((), (), s32[]{:S(2)}) async-start(), calls=%async_computation.5 | async-start | bytes 5898240 | tf_op jit(solution)/shard_map/all_gather | solution.py:77
  134.3 93.4 %copy-start.6 = (bf16[1,2048,256]{2,1,0:T(8,128)(2,1)S(1)}, bf16[1,2048,256]{2,1,0:T(8,128)(2,1)}, u32[]{:S(2)}) copy-start(bf16[1,2048,256]{2,1,0:T(8,128)(2,1)} %param.15) | copy-start | bytes 3145732
  175.1 56.6 %copy-start.7 = (bf16[1,2048,256]{2,1,0:T(8,128)(2,1)S(1)}, bf16[1,2048,256]{2,1,0:T(8,128)(2,1)}, u32[]{:S(2)}) copy-start(bf16[1,2048,256]{2,1,0:T(8,128)(2,1)} %param.16) | copy-start | bytes 3145732
  227.8 3.9 copy-start.5
  233.2 35.2 %copy-start.1 = (bf16[1152,256]{1,0:T(8,128)(2,1)}, bf16[1152,256]{1,0:T(8,128)(2,1)S(1)}, u32[]{:S(2)}) copy-start(bf16[1152,256]{1,0:T(8,128)(2,1)S(1)} %fusion) | copy-start | bytes 1769476
  233.2 18.0 %collective-permute-start = (bf16[1152,256]{1,0:T(8,128)(2,1)S(1)}, bf16[1152,256]{1,0:T(8,128)(2,1)S(1)}, u32[]{:S(2)}, u32[]{:S(2)}) collective-permute-start(bf16[1152,256]{1,0:T(8,128)(2,1)S(1)} %fusion), channel_id=1, source_target_pairs={{0,1},{1,2},{2,3},{3,0},{4,5},{5,6},{6,7},{7,4},{8,9},{9,10},{10,1... | collective-permute-start | bytes 1769480 | tf_op jit(solution)/shard_map/ppermute | solution.py:87
  236.1 17.2 %collective-permute-start.2 = (bf16[1152,256]{1,0:T(8,128)(2,1)S(1)}, bf16[1152,256]{1,0:T(8,128)(2,1)S(1)}, u32[]{:S(2)}, u32[]{:S(2)}) collective-permute-start(bf16[1152,256]{1,0:T(8,128)(2,1)S(1)} %fusion), channel_id=1, source_target_pairs={{1,0},{2,1},{3,2},{0,3},{5,4},{6,5},{7,6},{4,7},{9,8},{10,9},{11,1... | collective-permute-start | bytes 1769480 | tf_op jit(solution)/shard_map/ppermute | solution.py:89
  251.3 17.2 %copy-start.2 = (bf16[1152,256]{1,0:T(8,128)(2,1)}, bf16[1152,256]{1,0:T(8,128)(2,1)S(1)}, u32[]{:S(2)}) copy-start(bf16[1152,256]{1,0:T(8,128)(2,1)S(1)} %collective-permute-done) | copy-start | bytes 1769476
  251.3 17.2 %collective-permute-start.1 = (bf16[1152,256]{1,0:T(8,128)(2,1)S(1)}, bf16[1152,256]{1,0:T(8,128)(2,1)S(1)}, u32[]{:S(2)}, u32[]{:S(2)}) collective-permute-start(bf16[1152,256]{1,0:T(8,128)(2,1)S(1)} %collective-permute-done), channel_id=1, source_target_pairs={{0,1},{1,2},{2,3},{3,0},{4,5},{5,6},{6,7},{7,4},{8,9},{9,10},{10,1... | collective-permute-start | bytes 1769480 | tf_op jit(solution)/shard_map/ppermute | solution.py:87
  253.3 15.2 %copy-start.3 = (bf16[1152,256]{1,0:T(8,128)(2,1)}, bf16[1152,256]{1,0:T(8,128)(2,1)S(1)}, u32[]{:S(2)}) copy-start(bf16[1152,256]{1,0:T(8,128)(2,1)S(1)} %collective-permute-done.2) | copy-start | bytes 1769476
  268.5 0.8 copy-start.4
  278.8 31.2 %all-to-all-start.3 = ((bf16[8,144,512]{2,1,0:T(8,128)(2,1)}), bf16[8,144,512]{2,1,0:T(8,128)(2,1)S(1)}, u32[]{:S(2)}, u32[]{:S(2)}) async-start(bf16[8,144,512]{2,1,0:T(8,128)(2,1)} %bitcast.60), calls=%async_computation.3 | async-start | bytes 2359296 | tf_op jit(solution)/shard_map/all_to_all | solution.py:95
Sparse Core Ops, SparseCore 0:
  175.2 52.4 all-gather.3
